TPU v7x, 32 devices: a whole 2x2x4 slice. The times are simulated.
32 devices in a mesh: grp: 2 (over y), sp: 4 (over z), tp: 4 (over x, core).
Axes of the slice: x: 2, y: 2, z: 4, core: 2. Of those that a mesh axis runs over, the one named last changes fastest.
Arguments:
- prompt_rows: bfloat16 [6144, 2048], P(('grp', 'sp')), parts along dimension 0, may hold values from -6 to 6
- norm_gain: float32 [2048], replicated, may hold values from 0.1 to 1.9
- key_weight: bfloat16 [2048, 1024], P(None, 'tp'), may hold values from -0.125 to 0.125
- value_weight: bfloat16 [2048, 1024], P(None, 'tp'), may hold values from -0.125 to 0.125
- new_query: bfloat16 [2048], P(('grp', 'tp')), parts along dimension 0, may hold values from -6 to 6
- score_offset: float32 [16], P('tp'), may hold values from -11.5 to -4
- output_gain: float32 [1024], P('tp'), may hold values from 0.1 to 1.9
Outputs:
- key_cache: bfloat16 [8, 4, 4, 768, 64], P(('grp', 'tp'), 'sp'), parts along dimension 0
- value_cache: bfloat16 [8, 4, 4, 768, 64], P(('grp', 'tp'), 'sp'), parts along dimension 0
- first_read: bfloat16 [2048], P(('grp', 'tp')), parts along dimension 0
There are 2 independent parts, one for each index of `grp`. A program takes and returns all parts, laid end to end along the dimension named above; an argument that names none is the same for every part. Nothing has to cross between parts.
All inputs are finite; a program needn't handle non-finite values.
Results may differ from a plain program's by a relative error of at most 0.0059.
Values may be sent and summed in bfloat16 or wider, within the bound.
A program may use at most 64 MiB of HBM per device.

v0:
```python
import jax
import jax.numpy as jnp
from jax import lax
from jax.sharding import PartitionSpec as P

EPSILON = 1e-06


def prefix(value, axis, combine, identity):
    peers, position = (lax.axis_size(axis), lax.axis_index(axis))
    everything = lax.all_gather(value, axis)
    start = jnp.broadcast_to(jnp.asarray(identity, value.dtype), value.shape)

    def hop(k, before):
        at = peers - 1 - k
        reached = at > position
        new = combine(before, everything[at])
        return jnp.where(reached, new, before)

    return lax.fori_loop(0, peers, hop, start)


def normalize(rows, norm_gain):
    rows32 = rows.astype(jnp.float32)
    mean_square = jnp.mean(rows32 * rows32, axis=-1, keepdims=True)
    return (rows32 * lax.rsqrt(mean_square + EPSILON) * norm_gain).astype(jnp.bfloat16)


def project_rows(rows, norm_gain, key_weight, value_weight):
    normed = normalize(rows, norm_gain)
    keys = jnp.dot(normed, key_weight, preferred_element_type=jnp.float32).astype(jnp.bfloat16)
    values = jnp.dot(normed, value_weight, preferred_element_type=jnp.float32).astype(jnp.bfloat16)
    return (keys, values)


def cache_layout(keys, values, head_count):
    devices = lax.axis_size("sp")
    subs = devices // head_count
    depth = keys.shape[1] // head_count
    rows = keys.shape[0] // subs

    def arrange(cache):
        split = cache.reshape(subs, rows, head_count, depth)
        return jnp.transpose(split, (2, 0, 1, 3)).reshape(devices, 1, rows, depth)

    moved_keys, moved_values = (
        lax.all_to_all(arrange(keys), "sp", split_axis=0, concat_axis=1, tiled=True),
        lax.all_to_all(arrange(values), "sp", split_axis=0, concat_axis=1, tiled=True),
    )
    target = (1, 1, devices, rows, depth)
    return (moved_keys.reshape(target), moved_values.reshape(target))


def add_terms(first_part, second_part):
    return first_part + second_part


def read_early(new_query, keys, values, score_offset):
    head_count = score_offset.shape[0]
    depth = keys.shape[1] // head_count
    query2 = new_query.reshape(head_count, depth)
    keys3 = keys.reshape(keys.shape[0], head_count, depth)
    scores = jnp.einsum("hd,shd->hs", query2, keys3, preferred_element_type=jnp.float32)
    scores = scores * depth ** (-0.5) + score_offset[:, None]
    remain = jax.nn.log_sigmoid(-scores)
    within = lax.cumsum(remain, axis=1, reverse=True) - remain
    totals = jnp.sum(remain, axis=1)
    beyond = prefix(totals, "sp", add_terms, jnp.zeros_like(totals))
    sticks = jnp.exp(jax.nn.log_sigmoid(scores) + within + beyond[:, None]).astype(jnp.bfloat16)
    values3 = values.reshape(values.shape[0], head_count, depth)
    partial_value = jnp.einsum("hs,shd->hd", sticks, values3, preferred_element_type=jnp.float32)
    return lax.psum(partial_value, "sp")


def finish_read(mixed, output_gain, head_count):
    spread = jnp.mean(mixed * mixed, axis=-1, keepdims=True)
    result = mixed * lax.rsqrt(spread + EPSILON) * output_gain.reshape(head_count, -1)
    return result.reshape(-1).astype(jnp.bfloat16)


def body(prompt_rows, norm_gain, key_weight, value_weight, new_query, score_offset, output_gain):
    head_count = score_offset.shape[0]
    keys_here, values_here = project_rows(prompt_rows, norm_gain, key_weight, value_weight)
    keys_all, values_all = cache_layout(keys_here, values_here, head_count)
    local_keys, local_values = project_rows(prompt_rows, norm_gain, key_weight, value_weight)
    mixed = read_early(new_query, local_keys, local_values, score_offset)
    return (keys_all, values_all, finish_read(mixed, output_gain, head_count))


def solution(mesh):
    in_specs = (
        P(("grp", "sp"), None),
        P(),
        P(None, "tp"),
        P(None, "tp"),
        P(("grp", "tp")),
        P("tp"),
        P("tp"),
    )
    out_specs = (
        P(("grp", "tp"), "sp", None, None, None),
        P(("grp", "tp"), "sp", None, None, None),
        P(("grp", "tp")),
    )
    return jax.shard_map(body, mesh=mesh, in_specs=in_specs, out_specs=out_specs, check_vma=False)
```

profile of v0, /device:TPU:0, one launch (start us, length us, event | category | flops | bytes accessed | tf_op | source)
XLA Modules:
  0.0 56.2 jit_solution(451119704450405001)
XLA Ops:
  0.6 0.0 copy-start
  0.6 0.0 copy-start.1
  0.7 0.0 copy-start.6
  0.7 2.7 %fusion = f32[768]{0:T(1024)S(1)} fusion(bf16[768,2048]{1,0:T(8,128)(2,1)} %param.9), kind=kLoop, calls=%fused_computation.4 | loop fusion | flops 4717824 | bytes 3148800 | tf_op jit(solution)/shard_map/reduce_sum | solution.py:25
  3.4 0.0 copy-done
  3.4 0.4 copy-done.1
  3.8 0.0 copy-done.6
  3.8 0.0 copy-start.4
  3.8 0.0 copy-start.2
  3.8 0.0 copy-start.7
  3.8 0.0 copy-start.5
  3.8 2.1 %convolution_convert_fusion.1 = bf16[768,256]{0,1:T(8,128)(2,1)} fusion(bf16[2048,256]{1,0:T(8,128)(2,1)S(1)} %copy-done, bf16[768,2048]{1,0:T(8,128)(2,1)S(1)} %copy-done.1, f32[2048]{0:T(1024)S(1)} %copy-done.6, f32[768]{0:T(1024)S(1)} %add_rsqrt_fusion), kind=kOutput, calls=%fused_computation.8 | convolution fusion | flops 811794432 | bytes 4598784 | tf_op jit(solution)/shard_map/dot_general | solution.py:31
  5.9 6.3 %all-to-all-start = ((bf16[4,1,768,64]{2,3,1,0:T(8,128)(2,1)}), bf16[4,1,768,64]{2,3,1,0:T(8,128)(2,1)S(1)}, u32[]{:S(2)}, u32[]{:S(2)}) async-start(bf16[4,1,768,64]{2,3,1,0:T(8,128)(2,1)} %bitcast.2), calls=%async_computation | async-start | bytes 786432 | tf_op jit(solution)/shard_map/all_to_all | solution.py:47
  12.3 0.0 copy-done.4
  12.3 0.1 reshape.98
  12.4 1.2 %fusion.16 = f32[4,1,768]{2,1,0:T(1,128)S(1)} fusion(bf16[768,4,64]{0,2,1:T(8,128)(2,1)} %bitcast.8, bf16[4,64,1]{1,2,0:T(2,128)(2,1)S(1)} %reshape.98), kind=kOutput, calls=%fused_computation.31 | convolution fusion | flops 393216 | bytes 406016 | tf_op jit(solution)/shard_map/hd,shd->hs/dot_general | solution.py:63
  13.5 0.0 copy-done.2
  13.5 0.2 fusion.15
  13.7 5.0 %reduce-window.6 = f32[4,6,128]{2,1,0:T(8,128)S(1)} reduce-window(f32[4,6,128]{2,1,0:T(8,128)S(1)} %reshape.83, f32[]{:T(128)} %constant.61.clone.1), window={size=1x1x128 pad=0_0x0_0x0_127}, to_apply=%region_1.0 | reduce-window | flops 390144 | bytes 24580 | tf_op jit(solution)/shard_map/reduce-window
  18.7 0.1 slice_reduce_fusion
  18.8 0.2 reduce-window.9
  19.0 0.1 slice.7
  19.1 0.1 add_bitcast_fusion
  19.1 0.0 copy-done.7
  19.1 0.6 %dynamic-slice = u32[1]{0:T(128)} dynamic-slice(u32[32]{0:T(128)S(1)} %copy-done.7, u32[]{:T(128)S(6)} %add.95), dynamic_slice_sizes={1} | dynamic-slice | bytes 12
  20.4 0.1 negate_dynamic-update-slice_fusion
  20.5 12.2 %all-reduce = f32[16]{0:T(128)S(1)} all-reduce(f32[16]{0:T(128)S(1)} %negate_dynamic-update-slice_fusion), channel_id=2, replica_groups=mesh['grp'=2,'sp'=4,'tp'=4] {'sp'}, use_global_device_ids=true, to_apply=%add | all-reduce | flops 16 | bytes 128
  32.6 0.1 reshape.87
  32.7 0.1 while.16
  32.9 0.1 fusion.13
  33.0 0.0 copy-done.5
  33.0 0.0 copy-start.3
  33.0 3.9 %convolution_convert_fusion = bf16[768,256]{0,1:T(8,128)(2,1)} fusion(bf16[2048,256]{1,0:T(8,128)(2,1)S(1)} %copy-done.5, bf16[768,2048]{1,0:T(8,128)(2,1)} %param.9, f32[2048]{0:T(1024)S(1)} %copy-done.6, f32[768]{0:T(1024)S(1)} %add_rsqrt_fusion), kind=kOutput, calls=%fused_computation.7 | convolution fusion | flops 811794432 | bytes 4598784 | tf_op jit(solution)/shard_map/dot_general | solution.py:32
  36.9 0.0 all-to-all-done
  36.9 3.5 %all-to-all-start.1 = ((bf16[4,1,768,64]{2,3,1,0:T(8,128)(2,1)}), bf16[4,1,768,64]{2,3,1,0:T(8,128)(2,1)S(1)}, u32[]{:S(2)}, u32[]{:S(2)}) async-start(bf16[4,1,768,64]{2,3,1,0:T(8,128)(2,1)} %bitcast.6), calls=%async_computation.1 | async-start | bytes 786432 | tf_op jit(solution)/shard_map/all_to_all | solution.py:48
  40.4 1.2 %fusion.11 = f32[4,1,64]{2,1,0:T(1,128)S(1)} fusion(bf16[768,4,64]{0,2,1:T(8,128)(2,1)} %bitcast.12, bf16[4,768,1]{1,0,2:T(4,128)(2,1)S(1)} %fusion.13), kind=kOutput, calls=%fused_computation.21 | convolution fusion | flops 393216 | bytes 400384 | tf_op jit(solution)/shard_map/hs,shd->hd/dot_general | solution.py:71
  41.6 0.0 copy-done.3
  41.6 0.1 reshape.86
  41.7 12.1 %psum.7 = f32[4,64]{1,0:T(4,128)S(1)} all-reduce(f32[4,64]{1,0:T(4,128)S(1)} %bitcast.54), channel_id=1, replica_groups=mesh['grp'=2,'sp'=4,'tp'=4] {'sp'}, use_global_device_ids=true, to_apply=%region_6.7 | all-reduce | flops 256 | bytes 2048 | tf_op jit(solution)/shard_map/psum | solution.py:72
  53.9 0.1 multiply_reduce_fusion
  54.0 0.1 multiply_convert_fusion
  54.1 0.6 %convert_element_type.31 = bf16[256]{0:T(256)(128)(2,1)} reshape(bf16[4,64]{1,0:T(4,128)(2,1)S(1)} %multiply_convert_fusion) | data formatting | bytes 1024 | tf_op jit(solution)/shard_map/convert_element_type | solution.py:78
  54.7 0.0 all-to-all-done.1
  54.7 0.7 %copy.46 = bf16[1,1,4,768,64]{3,4,2,1,0:T(8,128)(2,1)} copy(bf16[1,1,4,768,64]{3,4,2,1,0:T(8,128)(2,1)S(1)} %bitcast.52) | data formatting | bytes 786432
  55.4 0.7 %copy.47 = bf16[1,1,4,768,64]{3,4,2,1,0:T(8,128)(2,1)} copy(bf16[1,1,4,768,64]{3,4,2,1,0:T(8,128)(2,1)S(1)} %bitcast.53) | data formatting | bytes 786432
  (9 shorter events, 0.1 us)
Async XLA Ops:
  0.6 2.8 %copy-start = (bf16[2048,256]{1,0:T(8,128)(2,1)S(1)}, bf16[2048,256]{1,0:T(8,128)(2,1)}, u32[]{:S(2)}) copy-start(bf16[2048,256]{1,0:T(8,128)(2,1)} %param.11) | copy-start | bytes 3145732
  0.6 3.2 %copy-start.1 = (bf16[768,2048]{1,0:T(8,128)(2,1)S(1)}, bf16[768,2048]{1,0:T(8,128)(2,1)}, u32[]{:S(2)}) copy-start(bf16[768,2048]{1,0:T(8,128)(2,1)} %param.9) | copy-start | bytes 9437188
  0.7 3.1 %copy-start.6 = (f32[2048]{0:T(1024)S(1)}, f32[2048]{0:T(1024)}, u32[]{:S(2)}) copy-start(f32[2048]{0:T(1024)} %param.10) | copy-start | bytes 24580
  3.8 8.5 %copy-start.4 = (bf16[256]{0:T(256)(128)(2,1)S(1)}, bf16[256]{0:T(256)(128)(2,1)}, u32[]{:S(2)}) copy-start(bf16[256]{0:T(256)(128)(2,1)} %param.13) | copy-start | bytes 1540
  3.8 9.7 %copy-start.2 = (f32[4]{0:T(128)S(1)}, f32[4]{0:T(128)}, u32[]{:S(2)}) copy-start(f32[4]{0:T(128)} %param.14) | copy-start | bytes 52
  3.8 15.3 %copy-start.7 = (u32[32]{0:T(128)S(1)}, u32[32]{0:T(128)}, u32[]{:S(2)}) copy-start(u32[32]{0:T(128)} %constant.71) | copy-start | bytes 388
  3.8 29.2 %copy-start.5 = (bf16[2048,256]{1,0:T(8,128)(2,1)S(1)}, bf16[2048,256]{1,0:T(8,128)(2,1)}, u32[]{:S(2)}) copy-start(bf16[2048,256]{1,0:T(8,128)(2,1)} %param.12) | copy-start | bytes 3145732
  5.9 31.0 %all-to-all-start = ((bf16[4,1,768,64]{2,3,1,0:T(8,128)(2,1)}), bf16[4,1,768,64]{2,3,1,0:T(8,128)(2,1)S(1)}, u32[]{:S(2)}, u32[]{:S(2)}) async-start(bf16[4,1,768,64]{2,3,1,0:T(8,128)(2,1)} %bitcast.2), calls=%async_computation | async-start | bytes 786432 | tf_op jit(solution)/shard_map/all_to_all | solution.py:47
  33.0 8.6 %copy-start.3 = (f32[256]{0:T(256)S(1)}, f32[256]{0:T(256)}, u32[]{:S(2)}) copy-start(f32[256]{0:T(256)} %param.15) | copy-start | bytes 3076
  36.9 17.7 %all-to-all-start.1 = ((bf16[4,1,768,64]{2,3,1,0:T(8,128)(2,1)}), bf16[4,1,768,64]{2,3,1,0:T(8,128)(2,1)S(1)}, u32[]{:S(2)}, u32[]{:S(2)}) async-start(bf16[4,1,768,64]{2,3,1,0:T(8,128)(2,1)} %bitcast.6), calls=%async_computation.1 | async-start | bytes 786432 | tf_op jit(solution)/shard_map/all_to_all | solution.py:48
where the time goes:
time: 56.6 us; the launch traced here: 56.2 us
  blocking collectives  24.3 us (43%)
  starting transfers between devices  9.81 us (17%)
  other arithmetic  8.65 us (15%)
  matrix products  8.39 us (15%)
  local copies, waits for them, and re-layouts  3.53 us (6%)
  between operations  1.39 us (2%)
    unnamed x1, blocking collectives  12.2 us
    psum x1, blocking collectives, read_early(): return lax.psum(partial_value, 'sp')  12.1 us
    all_to_all x1, starting transfers between devices, cache_layout(): lax.all_to_all(arrange(keys), 'sp', split_axis=0, concat_axis=1, tiled=True)  6.35 us
    another operation x2, other arithmetic  5.16 us
    dot_general x1, matrix products, project_rows(): jnp.dot(normed, value_weight, preferred_element_type=jnp.float32)  3.9 us
    all_to_all x1, starting transfers between devices, cache_layout(): lax.all_to_all(arrange(values), 'sp', split_axis=0, concat_axis=1, tiled=...  3.46 us
    reduce_sum x1, other arithmetic, normalize(): mean_square = jnp.mean(rows32 * rows32, axis=-1, keepdims=True)  2.72 us
    unnamed x20, local copies, waits for them, and re-layouts  2.51 us
  transfers between devices with their start and end apart: 2, of which 0 were waited for; matrix products, arithmetic and copies ran while one was open for 25% of the time, Pallas kernels for 0%

commit v1 on v0

--- a/solution.py
+++ b/solution.py
@@ -1,6 +1,10 @@
+import functools
+
 import jax
 import jax.numpy as jnp
 from jax import lax
+from jax.experimental import pallas as pl
+from jax.experimental.pallas import tpu as pltpu
 from jax.sharding import PartitionSpec as P
 
 EPSILON = 1e-06
@@ -78,13 +82,240 @@
     return result.reshape(-1).astype(jnp.bfloat16)
 
 
-def body(prompt_rows, norm_gain, key_weight, value_weight, new_query, score_offset, output_gain):
+LANES = 128
+VMEM_BYTES = 67043328
+ROW_SLOTS = 8
+MESH = pl.DeviceIdType.MESH
+
+
+def chunk_rows(rows):
+    return next(size for size in (2 * LANES, LANES) if rows % size == 0)
+
+
+def fused_kernel(
+    peers, x_hbm, gain_hbm, wk_hbm, wv_hbm, query_hbm, offset_hbm, out_gain_hbm,
+    key_out, value_out, read_out,
+    x, gain, wk, wv, query, offset, out_gain, kv, outbox, inbox,
+    x_sem, in_sem, send_sem, recv_sem, own_sem, small_send, small_recv,
+):
+    rows = x.shape[0]
+    width = wk.shape[1]
+    chunk = kv.shape[3]
+    chunks = rows // chunk
+    depth = width // peers
+    me = lax.axis_index("sp")
+    f32, bf16 = jnp.float32, jnp.bfloat16
+
+    def part(c):
+        return pl.ds(c * chunk, chunk)
+
+    loads = [
+        pltpu.make_async_copy(src, dst, in_sem.at[i])
+        for i, (src, dst) in enumerate(
+            ((gain_hbm, gain), (wk_hbm, wk), (wv_hbm, wv), (query_hbm, query), (offset_hbm, offset), (out_gain_hbm, out_gain))
+        )
+    ]
+    x_loads = [pltpu.make_async_copy(x_hbm.at[part(c), :], x.at[part(c), :], x_sem.at[c]) for c in range(chunks)]
+    loads[0].start()
+    x_loads[0].start()
+    loads[1].start()
+    loads[2].start()
+    for copy in x_loads[1:] + loads[3:]:
+        copy.start()
+
+    barrier = pltpu.get_barrier_semaphore()
+    others = [lax.rem(me + d, peers) for d in range(1, peers)]
+    for peer in others:
+        pl.semaphore_signal(barrier, inc=1, device_id={"sp": peer}, device_id_type=MESH)
+
+    outs = (key_out, value_out)
+    order = sorted(range(1, peers), key=lambda d: -min(d, peers - d))
+
+    def send(kind, c, d):
+        peer = lax.rem(me + d, peers)
+        return pltpu.make_async_remote_copy(
+            src_ref=kv.at[kind, c, pl.ds(pl.multiple_of(peer * depth, depth), depth), :],
+            dst_ref=outs[kind].at[me, :, part(c)],
+            send_sem=send_sem.at[kind, c, d - 1],
+            recv_sem=recv_sem.at[kind, c, d - 1],
+            device_id={"sp": peer},
+            device_id_type=MESH,
+        )
+
+    def keep(kind, c):
+        return pltpu.make_async_copy(
+            kv.at[kind, c, pl.ds(pl.multiple_of(me * depth, depth), depth), :],
+            outs[kind].at[me, :, part(c)],
+            own_sem.at[kind, c],
+        )
+
+    def send_all(c):
+        for d in order:
+            send(0, c, d).start()
+            send(1, c, d).start()
+        keep(0, c).start()
+        keep(1, c).start()
+
+    loads[0].wait()
+    gain_row = gain[...].reshape(1, -1)
+    for c in range(chunks):
+        x_loads[c].wait()
+        x32 = x[part(c), :].astype(f32)
+        mean_square = jnp.mean(x32 * x32, axis=-1, keepdims=True)
+        normed = (x32 * lax.rsqrt(mean_square + EPSILON) * gain_row).astype(bf16)
+        for kind, weight in ((0, wk), (1, wv)):
+            if c == 0:
+                loads[1 + kind].wait()
+            product = jnp.dot(normed, weight[...], preferred_element_type=f32)
+            kv[kind, c] = product.T.astype(bf16)
+        if c == 0:
+            pl.semaphore_wait(barrier, peers - 1)
+        if c < chunks - 1:
+            send_all(c)
+
+    for copy in loads[3:]:
+        copy.wait()
+    head_of = lax.broadcasted_iota(jnp.int32, (ROW_SLOTS, width), 1) // depth
+    mine = head_of == lax.broadcasted_iota(jnp.int32, (ROW_SLOTS, width), 0)
+    query_rows = jnp.where(mine, query[...].astype(f32).reshape(1, -1), 0.0).astype(bf16)
+    slot = lax.broadcasted_iota(jnp.int32, (ROW_SLOTS, 1), 0)
+    shift = jnp.zeros((ROW_SLOTS, 1), f32)
+    for h in range(peers):
+        shift = jnp.where(slot == h, offset[h], shift)
+    scores = [
+        jnp.dot(query_rows, kv[0, c], preferred_element_type=f32) * depth ** (-0.5) + shift for c in range(chunks)
+    ]
+    tiles = [s[:, t * LANES:(t + 1) * LANES] for s in scores for t in range(chunk // LANES)]
+    stacked = jnp.concatenate(tiles, axis=0)
+    tail = jnp.log1p(jnp.exp(-jnp.abs(stacked)))
+    remain = -jnp.maximum(stacked, 0.0) - tail
+    later = lax.broadcasted_iota(jnp.int32, (LANES, LANES), 0) > lax.broadcasted_iota(jnp.int32, (LANES, LANES), 1)
+    within = jnp.dot(remain, later.astype(f32), precision=lax.Precision.HIGHEST, preferred_element_type=f32)
+    sums = jnp.sum(remain, axis=1, keepdims=True)
+    running = jnp.zeros((ROW_SLOTS, 1), f32)
+    beyond = [None] * len(tiles)
+    for t in reversed(range(len(tiles))):
+        beyond[t] = running
+        running = running + sums[t * ROW_SLOTS:(t + 1) * ROW_SLOTS]
+    sticks = jnp.exp(jnp.minimum(stacked, 0.0) - tail + within + jnp.concatenate(beyond, axis=0)).astype(bf16)
+    partial = jnp.zeros((ROW_SLOTS, width), f32)
+    per = chunk // LANES
+    for c in range(chunks):
+        block = jnp.concatenate(
+            [sticks[(c * per + t) * ROW_SLOTS:(c * per + t + 1) * ROW_SLOTS] for t in range(per)], axis=1
+        )
+        partial = partial + lax.dot_general(
+            block, kv[1, c], (((1,), (1,)), ((), ())), preferred_element_type=f32
+        )
+    zeros = jnp.zeros((ROW_SLOTS, width), f32)
+    outbox[0:1, :] = jnp.sum(jnp.where(mine, partial, zeros), axis=0, keepdims=True)
+    outbox[1:2, :] = jnp.sum(jnp.where(mine, running, zeros), axis=0, keepdims=True)
+
+    def post(d):
+        return pltpu.make_async_remote_copy(
+            src_ref=outbox,
+            dst_ref=inbox.at[d],
+            send_sem=small_send.at[d - 1],
+            recv_sem=small_recv.at[d - 1],
+            device_id={"sp": lax.rem(me + d, peers)},
+            device_id_type=MESH,
+        )
+
+    for d in order:
+        post(d).start()
+    send_all(chunks - 1)
+
+    for d in range(1, peers):
+        post(d).wait_recv()
+    totals, values = [outbox[1:2, :]], [outbox[0:1, :]]
+    for d in range(1, peers):
+        totals.append(inbox[d, 1:2, :])
+        values.append(inbox[d, 0:1, :])
+    places = [lax.rem(me - d + peers, peers) for d in range(peers)]
+    mixed = jnp.zeros((1, width), f32)
+    for d in range(peers):
+        after = jnp.zeros((1, width), f32)
+        for e in range(peers):
+            if e != d:
+                after = after + jnp.where(places[e] > places[d], totals[e], 0.0)
+        mixed = mixed + values[d] * jnp.exp(after)
+    spread = jnp.sum(jnp.where(mine, mixed * mixed, zeros), axis=1, keepdims=True) * (1.0 / depth)
+    scale = jnp.sum(jnp.where(mine, lax.rsqrt(spread + EPSILON), zeros), axis=0, keepdims=True)
+    read_out[...] = (mixed * scale * out_gain[...].reshape(1, -1)).astype(bf16).reshape(read_out.shape)
+
+    for d in order:
+        post(d).wait_send()
+    for c in range(chunks):
+        for kind in range(2):
+            keep(kind, c).wait()
+            for d in order:
+                send(kind, c, d).wait()
+
+
+def fused_body(prompt_rows, norm_gain, key_weight, value_weight, new_query, score_offset, output_gain):
+    peers = lax.axis_size("sp")
+    rows, features = prompt_rows.shape
+    width = key_weight.shape[1]
+    depth = width // peers
+    chunk = chunk_rows(rows)
+    chunks = rows // chunk
+    f32, bf16 = jnp.float32, jnp.bfloat16
+    vmem = pl.BlockSpec(memory_space=pltpu.VMEM)
+    vmem_left = VMEM_BYTES - 2 * peers * depth * rows * 2 - 8192
+    dma = pltpu.SemaphoreType.DMA
+    cache = jax.ShapeDtypeStruct((peers, depth, rows), bf16)
+    keys, values, read = pl.pallas_call(
+        functools.partial(fused_kernel, peers),
+        out_shape=(cache, cache, jax.ShapeDtypeStruct((width,), bf16)),
+        in_specs=[pl.BlockSpec(memory_space=pltpu.HBM)] * 7,
+        out_specs=(vmem, vmem, vmem),
+        scratch_shapes=[
+            pltpu.VMEM((rows, features), bf16),
+            pltpu.VMEM((features,), f32),
+            pltpu.VMEM((features, width), bf16),
+            pltpu.VMEM((features, width), bf16),
+            pltpu.VMEM((width,), bf16),
+            pltpu.SMEM(score_offset.shape, f32),
+            pltpu.VMEM((width,), f32),
+            pltpu.VMEM((2, chunks, width, chunk), bf16),
+            pltpu.VMEM((2, width), f32),
+            pltpu.VMEM((peers, 2, width), f32),
+            dma((chunks,)),
+            dma((6,)),
+            dma((2, chunks, peers - 1)),
+            dma((2, chunks, peers - 1)),
+            dma((2, chunks)),
+            dma((peers - 1,)),
+            dma((peers - 1,)),
+        ],
+        compiler_params=pltpu.CompilerParams(
+            collective_id=0, has_side_effects=True, vmem_limit_bytes=vmem_left
+        ),
+        name="fused_cache_read",
+    )(prompt_rows, norm_gain, key_weight, value_weight, new_query, score_offset, output_gain)
+
+    def arrange(cache):
+        return jnp.swapaxes(cache, 1, 2).reshape(1, 1, peers, rows, depth)
+
+    return (arrange(keys), arrange(values), read)
+
+
+def plain_body(prompt_rows, norm_gain, key_weight, value_weight, new_query, score_offset, output_gain):
     head_count = score_offset.shape[0]
     keys_here, values_here = project_rows(prompt_rows, norm_gain, key_weight, value_weight)
     keys_all, values_all = cache_layout(keys_here, values_here, head_count)
     local_keys, local_values = project_rows(prompt_rows, norm_gain, key_weight, value_weight)
     mixed = read_early(new_query, local_keys, local_values, score_offset)
     return (keys_all, values_all, finish_read(mixed, output_gain, head_count))
+
+
+def body(prompt_rows, norm_gain, key_weight, value_weight, new_query, score_offset, output_gain):
+    arguments = (prompt_rows, norm_gain, key_weight, value_weight, new_query, score_offset, output_gain)
+    heads, devices = score_offset.shape[0], lax.axis_size("sp")
+    rows, depth = prompt_rows.shape[0], key_weight.shape[1] // heads
+    if heads == devices and heads <= 8 and rows % LANES == 0 and depth % 16 == 0 and key_weight.shape[1] % LANES == 0:
+        return fused_body(*arguments)
+    return plain_body(*arguments)
 
 
 def solution(mesh):

time: 56.6 us -> 31.8 us (0.56)
  Pallas kernels: 0 us -> 26.3 us
  blocking collectives: 24.3 us -> 0 us
  starting transfers between devices: 9.81 us -> 0 us
  other arithmetic: 8.65 us -> 0 us
  matrix products: 8.39 us -> 0 us
  local copies, waits for them, and re-layouts: 3.53 us -> 4.62 us
  between operations: 1.39 us -> 0.64 us
    pallas_call x0 -> x1, Pallas kernels: none -> 26.3 us  [fused_body(): pl.pallas_call(functools.partial(fused_kernel, peers), out_shape=(cache,...]
    unnamed x1 -> x0, blocking collectives: 12.2 us -> none
    psum x1 -> x0, blocking collectives: 12.1 us -> none  [read_early(): return lax.psum(partial_value, 'sp')]
    all_to_all x2 -> x0, starting transfers between devices: 9.81 us -> none  [the longest x1 6.35 us: cache_layout(): lax.all_to_all(arrange(keys), 'sp', split_axis=0, concat_axis=1, tiled=True)]
    dot_general x4 -> x0, matrix products: 8.39 us -> none  [the longest x1 3.9 us: project_rows(): jnp.dot(normed, value_weight, preferred_element_type=jnp.float32)]
    another operation x2 -> x0, other arithmetic: 5.16 us -> none
    reduce_sum x2 -> x0, other arithmetic: 2.84 us -> none  [the longest x1 2.72 us: normalize(): mean_square = jnp.mean(rows32 * rows32, axis=-1, keepdims=True)]
    unnamed x20 -> x3, local copies, waits for them, and re-layouts: 2.51 us -> 4.62 us
  transfers between devices with their start and end apart: 2 -> 0, of which waited for: 0 -> 0; matrix products, arithmetic and copies ran while one was open for 25% -> 0% of each run, Pallas kernels for 0% -> 0%
where the time goes in v1:
time: 31.8 us; the launch traced here: 31.5 us
  Pallas kernels  26.3 us (83%)
  local copies, waits for them, and re-layouts  4.62 us (15%)
  between operations  0.64 us (2%)
    pallas_call x1, Pallas kernels, fused_body(): pl.pallas_call(functools.partial(fused_kernel, peers), out_shape=(cache,...  26.3 us
    unnamed x3, local copies, waits for them, and re-layouts  4.62 us

profile of v1, /device:TPU:0, one launch (start us, length us, event | category | flops | bytes accessed | tf_op | source)
XLA Modules:
  0.0 31.5 jit_solution(11169448806986305431)
XLA Ops:
  0.6 26.3 %fused_cache_read.1 = (bf16[4,64,768]{2,1,0:T(8,128)(2,1)}, bf16[4,64,768]{2,1,0:T(8,128)(2,1)}, bf16[256]{0:T(256)(128)(2,1)}) custom-call(bf16[768,2048]{1,0:T(8,128)(2,1)} %x_hbm.1, f32[2048]{0:T(1024)} %gain_hbm.1, bf16[2048,256]{1,0:T(8,128)(2,1)} %wk_hbm.1, bf16[2048,256]{1,0:T(8,128)(2,1)} %wv_hbm.1, bf16[256]{0:T(256)(128)(2,1)} %query_hbm.1, ...), custom_call_target="tpu_custom_call" | custom-call | tf_op jit(solution)/shard_map/fused_cache_read/pallas_call | solution.py:267
  26.9 1.8 %copy.13 = bf16[1,1,4,768,64]{3,4,2,1,0:T(8,128)(2,1)} copy(bf16[1,1,4,768,64]{3,4,2,1,0:T(8,128)(2,1)} %bitcast.7) | data formatting | bytes 786432
  28.7 1.8 %copy.14 = bf16[1,1,4,768,64]{3,4,2,1,0:T(8,128)(2,1)} copy(bf16[1,1,4,768,64]{3,4,2,1,0:T(8,128)(2,1)} %bitcast.6) | data formatting | bytes 786432
  30.5 1.1 %copy.15 = bf16[256]{0:T(256)(128)(2,1)} copy(bf16[256]{0:T(256)(128)(2,1)} %get-tuple-element.14) | data formatting | bytes 1024

commit v2 on v1

--- a/solution.py
+++ b/solution.py
@@ -83,13 +83,18 @@
 
 
 LANES = 128
-VMEM_BYTES = 67043328
 ROW_SLOTS = 8
+VMEM_LIMIT = 40 * 1024 * 1024
 MESH = pl.DeviceIdType.MESH
 
 
-def chunk_rows(rows):
-    return next(size for size in (2 * LANES, LANES) if rows % size == 0)
+def row_chunks(rows):
+    sizes, left = [], rows
+    while left:
+        size = min((len(sizes) + 1) * LANES, left)
+        sizes.append(size)
+        left -= size
+    return [(sum(sizes[:i]), size) for i, size in enumerate(sizes)]
 
 
 def fused_kernel(
@@ -100,14 +105,14 @@
 ):
     rows = x.shape[0]
     width = wk.shape[1]
-    chunk = kv.shape[3]
-    chunks = rows // chunk
+    spans = row_chunks(rows)
+    chunks = len(spans)
     depth = width // peers
     me = lax.axis_index("sp")
     f32, bf16 = jnp.float32, jnp.bfloat16
 
     def part(c):
-        return pl.ds(c * chunk, chunk)
+        return pl.ds(*spans[c])
 
     loads = [
         pltpu.make_async_copy(src, dst, in_sem.at[i])
@@ -129,32 +134,49 @@
         pl.semaphore_signal(barrier, inc=1, device_id={"sp": peer}, device_id_type=MESH)
 
     outs = (key_out, value_out)
-    order = sorted(range(1, peers), key=lambda d: -min(d, peers - d))
-
-    def send(kind, c, d):
-        peer = lax.rem(me + d, peers)
+    left_half = 1 - (2 * me) // peers
+    targets = []
+    for j in range(peers - 1):
+        down, up = peers - 1 - j, j
+        down = down - (1 - (down - me + peers - 1) // peers)
+        up = up + (1 - (me - up + peers - 1) // peers)
+        targets.append(left_half * down + (1 - left_half) * up)
+
+    def head_rows(place):
+        return pl.ds(pl.multiple_of(place * depth, depth), depth)
+
+    def send(kind, c, j):
         return pltpu.make_async_remote_copy(
-            src_ref=kv.at[kind, c, pl.ds(pl.multiple_of(peer * depth, depth), depth), :],
+            src_ref=kv.at[kind, head_rows(targets[j]), part(c)],
             dst_ref=outs[kind].at[me, :, part(c)],
-            send_sem=send_sem.at[kind, c, d - 1],
-            recv_sem=recv_sem.at[kind, c, d - 1],
-            device_id={"sp": peer},
+            send_sem=send_sem.at[kind, c, j],
+            recv_sem=recv_sem.at[kind, c, me],
+            device_id={"sp": targets[j]},
+            device_id_type=MESH,
+        )
+
+    def arrival(kind, c, j):
+        return pltpu.make_async_remote_copy(
+            src_ref=kv.at[kind, head_rows(targets[j]), part(c)],
+            dst_ref=outs[kind].at[targets[j], :, part(c)],
+            send_sem=send_sem.at[kind, c, j],
+            recv_sem=recv_sem.at[kind, c, targets[j]],
+            device_id={"sp": targets[j]},
             device_id_type=MESH,
         )
 
     def keep(kind, c):
         return pltpu.make_async_copy(
-            kv.at[kind, c, pl.ds(pl.multiple_of(me * depth, depth), depth), :],
-            outs[kind].at[me, :, part(c)],
-            own_sem.at[kind, c],
-        )
-
-    def send_all(c):
-        for d in order:
-            send(0, c, d).start()
-            send(1, c, d).start()
-        keep(0, c).start()
-        keep(1, c).start()
+            kv.at[kind, head_rows(me), part(c)], outs[kind].at[me, :, part(c)], own_sem.at[kind, c]
+        )
+
+    def send_all(c, kinds=(0, 1)):
+        slots = range(peers - 1) if c < chunks - 1 else reversed(range(peers - 1))
+        for j in slots:
+            for kind in kinds:
+                send(kind, c, j).start()
+        for kind in kinds:
+            keep(kind, c).start()
 
     loads[0].wait()
     gain_row = gain[...].reshape(1, -1)
@@ -167,11 +189,11 @@
             if c == 0:
                 loads[1 + kind].wait()
             product = jnp.dot(normed, weight[...], preferred_element_type=f32)
-            kv[kind, c] = product.T.astype(bf16)
-        if c == 0:
-            pl.semaphore_wait(barrier, peers - 1)
-        if c < chunks - 1:
-            send_all(c)
+            kv[kind, :, part(c)] = product.T.astype(bf16)
+            if c == 0 and kind == 0:
+                pl.semaphore_wait(barrier, peers - 1)
+            if c < chunks - 1:
+                send_all(c, (kind,))
 
     for copy in loads[3:]:
         copy.wait()
@@ -182,10 +204,8 @@
     shift = jnp.zeros((ROW_SLOTS, 1), f32)
     for h in range(peers):
         shift = jnp.where(slot == h, offset[h], shift)
-    scores = [
-        jnp.dot(query_rows, kv[0, c], preferred_element_type=f32) * depth ** (-0.5) + shift for c in range(chunks)
-    ]
-    tiles = [s[:, t * LANES:(t + 1) * LANES] for s in scores for t in range(chunk // LANES)]
+    scores = jnp.dot(query_rows, kv[0], preferred_element_type=f32) * depth ** (-0.5) + shift
+    tiles = [scores[:, t * LANES:(t + 1) * LANES] for t in range(rows // LANES)]
     stacked = jnp.concatenate(tiles, axis=0)
     tail = jnp.log1p(jnp.exp(-jnp.abs(stacked)))
     remain = -jnp.maximum(stacked, 0.0) - tail
@@ -198,15 +218,8 @@
         beyond[t] = running
         running = running + sums[t * ROW_SLOTS:(t + 1) * ROW_SLOTS]
     sticks = jnp.exp(jnp.minimum(stacked, 0.0) - tail + within + jnp.concatenate(beyond, axis=0)).astype(bf16)
-    partial = jnp.zeros((ROW_SLOTS, width), f32)
-    per = chunk // LANES
-    for c in range(chunks):
-        block = jnp.concatenate(
-            [sticks[(c * per + t) * ROW_SLOTS:(c * per + t + 1) * ROW_SLOTS] for t in range(per)], axis=1
-        )
-        partial = partial + lax.dot_general(
-            block, kv[1, c], (((1,), (1,)), ((), ())), preferred_element_type=f32
-        )
+    sticks = jnp.concatenate([sticks[t * ROW_SLOTS:(t + 1) * ROW_SLOTS] for t in range(len(tiles))], axis=1)
+    partial = lax.dot_general(sticks, kv[1], (((1,), (1,)), ((), ())), preferred_element_type=f32)
     zeros = jnp.zeros((ROW_SLOTS, width), f32)
     outbox[0:1, :] = jnp.sum(jnp.where(mine, partial, zeros), axis=0, keepdims=True)
     outbox[1:2, :] = jnp.sum(jnp.where(mine, running, zeros), axis=0, keepdims=True)
@@ -221,7 +234,7 @@
             device_id_type=MESH,
         )
 
-    for d in order:
+    for d in range(1, peers):
         post(d).start()
     send_all(chunks - 1)
 
@@ -243,25 +256,51 @@
     scale = jnp.sum(jnp.where(mine, lax.rsqrt(spread + EPSILON), zeros), axis=0, keepdims=True)
     read_out[...] = (mixed * scale * out_gain[...].reshape(1, -1)).astype(bf16).reshape(read_out.shape)
 
-    for d in order:
+    for d in range(1, peers):
         post(d).wait_send()
     for c in range(chunks):
         for kind in range(2):
             keep(kind, c).wait()
-            for d in order:
-                send(kind, c, d).wait()
-
-
-def fused_body(prompt_rows, norm_gain, key_weight, value_weight, new_query, score_offset, output_gain):
+            for j in range(peers - 1):
+                send(kind, c, j).wait_send()
+                arrival(kind, c, j).wait_recv()
+
+
+def write_kernel(sources, targets, sems):
+    copies = [pltpu.make_async_copy(src, dst, sems.at[i]) for i, (src, dst) in enumerate(zip(sources, targets))]
+    for copy in copies:
+        copy.start()
+    for copy in copies:
+        copy.wait()
+
+
+def write_out(*arrays):
+    count = len(arrays)
+
+    def kernel(*refs):
+        write_kernel(refs[:count], refs[count:2 * count], refs[2 * count])
+
+    return pl.pallas_call(
+        kernel,
+        out_shape=tuple(jax.ShapeDtypeStruct(a.shape, a.dtype) for a in arrays),
+        in_specs=[pl.BlockSpec(memory_space=pltpu.VMEM)] * count,
+        out_specs=(pl.BlockSpec(memory_space=pltpu.HBM),) * count,
+        scratch_shapes=[pltpu.SemaphoreType.DMA((count,))],
+        compiler_params=pltpu.CompilerParams(vmem_limit_bytes=1024 * 1024),
+        name="write_out",
+    )(*arrays)
+
+
+def fused_body(*arguments):
+    prompt_rows, norm_gain, key_weight, value_weight, new_query, score_offset, output_gain = arguments
     peers = lax.axis_size("sp")
     rows, features = prompt_rows.shape
     width = key_weight.shape[1]
     depth = width // peers
-    chunk = chunk_rows(rows)
-    chunks = rows // chunk
+    chunks = len(row_chunks(rows))
     f32, bf16 = jnp.float32, jnp.bfloat16
     vmem = pl.BlockSpec(memory_space=pltpu.VMEM)
-    vmem_left = VMEM_BYTES - 2 * peers * depth * rows * 2 - 8192
+
     dma = pltpu.SemaphoreType.DMA
     cache = jax.ShapeDtypeStruct((peers, depth, rows), bf16)
     keys, values, read = pl.pallas_call(
@@ -277,22 +316,24 @@
             pltpu.VMEM((width,), bf16),
             pltpu.SMEM(score_offset.shape, f32),
             pltpu.VMEM((width,), f32),
-            pltpu.VMEM((2, chunks, width, chunk), bf16),
+            pltpu.VMEM((2, width, rows), bf16),
             pltpu.VMEM((2, width), f32),
             pltpu.VMEM((peers, 2, width), f32),
             dma((chunks,)),
             dma((6,)),
             dma((2, chunks, peers - 1)),
-            dma((2, chunks, peers - 1)),
+            dma((2, chunks, peers)),
             dma((2, chunks)),
             dma((peers - 1,)),
             dma((peers - 1,)),
         ],
         compiler_params=pltpu.CompilerParams(
-            collective_id=0, has_side_effects=True, vmem_limit_bytes=vmem_left
+            collective_id=0, has_side_effects=True, vmem_limit_bytes=VMEM_LIMIT
         ),
         name="fused_cache_read",
-    )(prompt_rows, norm_gain, key_weight, value_weight, new_query, score_offset, output_gain)
+    )(*[pltpu.with_memory_space_constraint(argument, pltpu.HBM) for argument in arguments])
+
+    keys, values, read = write_out(keys, values, read)
 
     def arrange(cache):
         return jnp.swapaxes(cache, 1, 2).reshape(1, 1, peers, rows, depth)

time: 31.8 us -> 26.7 us (0.84)
  local copies, waits for them, and re-layouts: 4.62 us -> 0 us
  Pallas kernels: 26.3 us -> 25.8 us
    unnamed x3 -> x0, local copies, waits for them, and re-layouts: 4.62 us -> none
    pallas_call x1, Pallas kernels: 26.3 us -> 24.9 us  [fused_body(): pl.pallas_call(functools.partial(fused_kernel, peers), out_shape=(cache,...]
    pallas_call x0 -> x1, Pallas kernels: none -> 0.91 us  [write_out(): pl.pallas_call(kernel, out_shape=tuple((jax.ShapeDtypeStruct(a.shape, a.d...]
where the time goes in v2:
time: 26.7 us; the launch traced here: 26.5 us
  Pallas kernels  25.8 us (97%)
  between operations  0.64 us (2%)
    pallas_call x1, Pallas kernels, fused_body(): pl.pallas_call(functools.partial(fused_kernel, peers), out_shape=(cache,...  24.9 us
    pallas_call x1, Pallas kernels, write_out(): pl.pallas_call(kernel, out_shape=tuple((jax.ShapeDtypeStruct(a.shape, a.d...  0.91 us

profile of v2, /device:TPU:0, one launch (start us, length us, event | category | flops | bytes accessed | tf_op | source)
XLA Modules:
  0.0 26.5 jit_solution(3283836601091374069)
XLA Ops:
  0.6 24.9 %fused_cache_read.1 = (bf16[4,64,768]{2,1,0:T(8,128)(2,1)S(1)}, bf16[4,64,768]{2,1,0:T(8,128)(2,1)S(1)}, bf16[256]{0:T(256)(128)(2,1)S(1)}) custom-call(bf16[768,2048]{1,0:T(8,128)(2,1)} %x_hbm.1, f32[2048]{0:T(1024)} %gain_hbm.1, bf16[2048,256]{1,0:T(8,128)(2,1)} %wk_hbm.1, bf16[2048,256]{1,0:T(8,128)(2,1)} %wv_hbm.1, bf16[256]{0:T(256)(128)(2,1)} %query_hbm.1, ...), custom_call_target="tpu_custom_call" | custom-call | tf_op jit(solution)/shard_map/fused_cache_read/pallas_call | solution.py:306
  25.6 0.9 %write_out.1 = (bf16[4,64,768]{2,1,0:T(8,128)(2,1)}, bf16[4,64,768]{2,1,0:T(8,128)(2,1)}, bf16[256]{0:T(256)(128)(2,1)}) custom-call(bf16[4,64,768]{2,1,0:T(8,128)(2,1)S(1)} %get-tuple-element.9.refs_0_, bf16[4,64,768]{2,1,0:T(8,128)(2,1)S(1)} %get-tuple-element.10.refs_1_, bf16[256]{0:T(256)(128)(2,1)S(1)} %get-tuple-element.11.refs_2_), custom_call_target="tpu_custom_call" | custom-call | tf_op jit(solution)/shard_map/write_out/pallas_call | solution.py:283

commit v3 on v2

--- a/solution.py
+++ b/solution.py
@@ -91,7 +91,7 @@
 def row_chunks(rows):
     sizes, left = [], rows
     while left:
-        size = min((len(sizes) + 1) * LANES, left)
+        size = LANES if len(sizes) < 2 else left
         sizes.append(size)
         left -= size
     return [(sum(sizes[:i]), size) for i, size in enumerate(sizes)]
@@ -111,6 +111,11 @@
     me = lax.axis_index("sp")
     f32, bf16 = jnp.float32, jnp.bfloat16
 
+    barrier = pltpu.get_barrier_semaphore()
+    others = [lax.rem(me + d, peers) for d in range(1, peers)]
+    for peer in others:
+        pl.semaphore_signal(barrier, inc=1, device_id={"sp": peer}, device_id_type=MESH)
+
     def part(c):
         return pl.ds(*spans[c])
 
@@ -121,17 +126,8 @@
         )
     ]
     x_loads = [pltpu.make_async_copy(x_hbm.at[part(c), :], x.at[part(c), :], x_sem.at[c]) for c in range(chunks)]
-    loads[0].start()
-    x_loads[0].start()
-    loads[1].start()
-    loads[2].start()
-    for copy in x_loads[1:] + loads[3:]:
+    for copy in (loads[1], x_loads[0], loads[0], loads[2]):
         copy.start()
-
-    barrier = pltpu.get_barrier_semaphore()
-    others = [lax.rem(me + d, peers) for d in range(1, peers)]
-    for peer in others:
-        pl.semaphore_signal(barrier, inc=1, device_id={"sp": peer}, device_id_type=MESH)
 
     outs = (key_out, value_out)
     left_half = 1 - (2 * me) // peers
@@ -171,8 +167,8 @@
         )
 
     def send_all(c, kinds=(0, 1)):
-        slots = range(peers - 1) if c < chunks - 1 else reversed(range(peers - 1))
-        for j in slots:
+        turn = 0 if c < chunks - 1 else peers // 2
+        for j in [(turn + i) % (peers - 1) for i in range(peers - 1)]:
             for kind in kinds:
                 send(kind, c, j).start()
         for kind in kinds:
@@ -182,6 +178,9 @@
     gain_row = gain[...].reshape(1, -1)
     for c in range(chunks):
         x_loads[c].wait()
+        if c == 0:
+            for copy in x_loads[1:] + loads[3:]:
+                copy.start()
         x32 = x[part(c), :].astype(f32)
         mean_square = jnp.mean(x32 * x32, axis=-1, keepdims=True)
         normed = (x32 * lax.rsqrt(mean_square + EPSILON) * gain_row).astype(bf16)

time: 26.7 us -> 24 us (0.90)
  Pallas kernels: 25.8 us -> 23.2 us
    pallas_call x1, Pallas kernels: 24.9 us -> 22.3 us  [fused_body(): pl.pallas_call(functools.partial(fused_kernel, peers), out_shape=(cache,...]
where the time goes in v3:
time: 24 us; the launch traced here: 23.8 us
  Pallas kernels  23.2 us (97%)
  between operations  0.64 us (3%)
    pallas_call x1, Pallas kernels, fused_body(): pl.pallas_call(functools.partial(fused_kernel, peers), out_shape=(cache,...  22.3 us
    pallas_call x1, Pallas kernels, write_out(): pl.pallas_call(kernel, out_shape=tuple((jax.ShapeDtypeStruct(a.shape, a.d...  0.91 us

profile of v3, /device:TPU:0, one launch (start us, length us, event | category | flops | bytes accessed | tf_op | source)
XLA Modules:
  0.0 23.8 jit_solution(4750349149054302699)
XLA Ops:
  0.6 22.3 %fused_cache_read.1 = (bf16[4,64,768]{2,1,0:T(8,128)(2,1)S(1)}, bf16[4,64,768]{2,1,0:T(8,128)(2,1)S(1)}, bf16[256]{0:T(256)(128)(2,1)S(1)}) custom-call(bf16[768,2048]{1,0:T(8,128)(2,1)} %x_hbm.1, f32[2048]{0:T(1024)} %gain_hbm.1, bf16[2048,256]{1,0:T(8,128)(2,1)} %wk_hbm.1, bf16[2048,256]{1,0:T(8,128)(2,1)} %wv_hbm.1, bf16[256]{0:T(256)(128)(2,1)} %query_hbm.1, ...), custom_call_target="tpu_custom_call" | custom-call | tf_op jit(solution)/shard_map/fused_cache_read/pallas_call | solution.py:305
  22.9 0.9 %write_out.1 = (bf16[4,64,768]{2,1,0:T(8,128)(2,1)}, bf16[4,64,768]{2,1,0:T(8,128)(2,1)}, bf16[256]{0:T(256)(128)(2,1)}) custom-call(bf16[4,64,768]{2,1,0:T(8,128)(2,1)S(1)} %get-tuple-element.9.refs_0_, bf16[4,64,768]{2,1,0:T(8,128)(2,1)S(1)} %get-tuple-element.10.refs_1_, bf16[256]{0:T(256)(128)(2,1)S(1)} %get-tuple-element.11.refs_2_), custom_call_target="tpu_custom_call" | custom-call | tf_op jit(solution)/shard_map/write_out/pallas_call | solution.py:282

commit v4 on v3

--- a/solution.py
+++ b/solution.py
@@ -91,7 +91,7 @@
 def row_chunks(rows):
     sizes, left = [], rows
     while left:
-        size = LANES if len(sizes) < 2 else left
+        size = LANES if not sizes else left
         sizes.append(size)
         left -= size
     return [(sum(sizes[:i]), size) for i, size in enumerate(sizes)]
@@ -166,13 +166,11 @@
             kv.at[kind, head_rows(me), part(c)], outs[kind].at[me, :, part(c)], own_sem.at[kind, c]
         )
 
-    def send_all(c, kinds=(0, 1)):
+    def send_all(c, kinds, pieces):
         turn = 0 if c < chunks - 1 else peers // 2
-        for j in [(turn + i) % (peers - 1) for i in range(peers - 1)]:
+        for j in [(turn + i) % (peers - 1) for i in pieces]:
             for kind in kinds:
                 send(kind, c, j).start()
-        for kind in kinds:
-            keep(kind, c).start()
 
     loads[0].wait()
     gain_row = gain[...].reshape(1, -1)
@@ -191,8 +189,8 @@
             kv[kind, :, part(c)] = product.T.astype(bf16)
             if c == 0 and kind == 0:
                 pl.semaphore_wait(barrier, peers - 1)
-            if c < chunks - 1:
-                send_all(c, (kind,))
+            send_all(c, (kind,), range(peers - 1 if c < chunks - 1 else peers - 2))
+            keep(kind, c).start()
 
     for copy in loads[3:]:
         copy.wait()
@@ -235,7 +233,7 @@
 
     for d in range(1, peers):
         post(d).start()
-    send_all(chunks - 1)
+    send_all(chunks - 1, (0, 1), (peers - 2,))
 
     for d in range(1, peers):
         post(d).wait_recv()

time: 24 us -> 23.9 us (level)
  the two profiles are of different devices: /device:TPU:0 before, /device:TPU:8 now
where the time goes in v4:
time: 23.9 us; the launch traced here: 23.7 us
  Pallas kernels  23.1 us (97%)
  between operations  0.64 us (3%)
    pallas_call x1, Pallas kernels, fused_body(): pl.pallas_call(functools.partial(fused_kernel, peers), out_shape=(cache,...  22.2 us
    pallas_call x1, Pallas kernels, write_out(): pl.pallas_call(kernel, out_shape=tuple((jax.ShapeDtypeStruct(a.shape, a.d...  0.91 us

profile of v4, /device:TPU:8, one launch (start us, length us, event | category | flops | bytes accessed | tf_op | source)
XLA Modules:
  0.0 23.7 jit_solution(10855974105799015313)
XLA Ops:
  0.6 22.2 %fused_cache_read.1 = (bf16[4,64,768]{2,1,0:T(8,128)(2,1)S(1)}, bf16[4,64,768]{2,1,0:T(8,128)(2,1)S(1)}, bf16[256]{0:T(256)(128)(2,1)S(1)}) custom-call(bf16[768,2048]{1,0:T(8,128)(2,1)} %x_hbm.1, f32[2048]{0:T(1024)} %gain_hbm.1, bf16[2048,256]{1,0:T(8,128)(2,1)} %wk_hbm.1, bf16[2048,256]{1,0:T(8,128)(2,1)} %wv_hbm.1, bf16[256]{0:T(256)(128)(2,1)} %query_hbm.1, ...), custom_call_target="tpu_custom_call" | custom-call | tf_op jit(solution)/shard_map/fused_cache_read/pallas_call | solution.py:303
  22.8 0.9 %write_out.1 = (bf16[4,64,768]{2,1,0:T(8,128)(2,1)}, bf16[4,64,768]{2,1,0:T(8,128)(2,1)}, bf16[256]{0:T(256)(128)(2,1)}) custom-call(bf16[4,64,768]{2,1,0:T(8,128)(2,1)S(1)} %get-tuple-element.9.refs_0_, bf16[4,64,768]{2,1,0:T(8,128)(2,1)S(1)} %get-tuple-element.10.refs_1_, bf16[256]{0:T(256)(128)(2,1)S(1)} %get-tuple-element.11.refs_2_), custom_call_target="tpu_custom_call" | custom-call | tf_op jit(solution)/shard_map/write_out/pallas_call | solution.py:280
